TPU v7x, 32 devices: a whole 2x2x4 slice. The times are simulated.
32 devices in a mesh: fs: 8 (over z, x), tp: 4 (over y, core).
Axes of the slice: x: 2, y: 2, z: 4, core: 2. Of those that a mesh axis runs over, the one named last changes fastest.
Arguments:
- tokens: bfloat16 [1024, 2048], P('fs'), may hold values from -6 to 6
- route_ids: int32 [1024, 2], P('fs'), may hold values from 0 to 15, as said below
- route_weights: float32 [1024, 2], P('fs'), may hold values from 0.05 to 0.6
- norm_gain: float32 [2048], P('fs'), may hold values from 0.1 to 1.9
- gate_weight: float32 [16, 2048, 1024], P(None, 'fs', 'tp'), may hold values from -6 to 6
- up_weight: float32 [16, 2048, 1024], P(None, 'fs', 'tp'), may hold values from -6 to 6
- down_weight: float32 [16, 2048, 1024], P(None, 'fs', 'tp'), may hold values from -6 to 6
Outputs:
- gate_served: bfloat16 [16, 2048, 1024], P('fs', None, 'tp')
- up_served: bfloat16 [16, 2048, 1024], P('fs', None, 'tp')
- down_served: bfloat16 [16, 2048, 1024], P('fs', None, 'tp')
- combined: bfloat16 [1024, 2048], P('fs', 'tp')
Inputs may be any that keep to these rules, and one draw needn't show every extreme that they name: `route_ids`: each row names 2 different experts of one group, numbers g * 4 to g * 4 + 3 for some g. In each aligned block of 128 rows (the rows of one index of fs) no expert is named by more than 32 rows, and some experts are named by exactly 32 rows in every block.
All inputs are finite; a program needn't handle non-finite values.
Results may differ from a plain program's by a relative error of at most 0.015.
Values may be sent and summed in bfloat16 or wider, within the bound.
A program may use at most 64 MiB of HBM per device.

v0:
```python
import jax
import jax.numpy as jnp
from jax import lax
from jax.sharding import PartitionSpec as P

GROUPS = 4


epsilon = 1e-06


def body(tokens, route_ids, route_weights, norm_gain, gate_weight, up_weight, down_weight):
    scaling = norm_gain[:, None]
    gate_folded = (scaling * gate_weight).astype(jnp.bfloat16)
    up_folded = (scaling * up_weight).astype(jnp.bfloat16)
    down_rounded = down_weight.astype(jnp.bfloat16)
    gate_served, up_served, down_served = (
        lax.all_to_all(gate_folded, "fs", split_axis=0, concat_axis=1, tiled=True),
        lax.all_to_all(up_folded, "fs", split_axis=0, concat_axis=1, tiled=True),
        lax.all_to_all(down_rounded, "fs", split_axis=0, concat_axis=1, tiled=True),
    )
    widened = tokens.astype(jnp.float32)
    normed = (
        widened * lax.rsqrt(jnp.mean(widened * widened, axis=1, keepdims=True) + epsilon)
    ).astype(jnp.bfloat16)
    tok_rows, d_model = tokens.shape
    routes = route_ids.shape[1]
    experts = gate_weight.shape[0]
    sources = lax.axis_size("fs")
    per_device = experts // sources
    capacity = tok_rows * GROUPS // experts
    flat_ids = route_ids.reshape(-1)
    onehot = (flat_ids[:, None] == jnp.arange(experts, dtype=jnp.int32)[None, :]).astype(jnp.int32)
    position = jnp.sum((jnp.cumsum(onehot, axis=0) - onehot) * onehot, axis=1)
    slot_index = (flat_ids * capacity + position).reshape(tok_rows, routes)
    token_of = jnp.repeat(jnp.arange(tok_rows, dtype=jnp.int32), routes)
    slot_token = (
        jnp.zeros((experts * capacity,), jnp.int32).at[slot_index.reshape(-1)].set(token_of)
    )
    hidden_local = gate_served.shape[2]
    col_width = d_model // lax.axis_size("tp")
    own_cols = lax.dynamic_slice_in_dim(normed, lax.axis_index("tp") * col_width, col_width, 1)
    arrived = lax.all_to_all(own_cols[slot_token], "fs", split_axis=0, concat_axis=0, tiled=True)
    arrived = arrived.reshape(sources, per_device, capacity, col_width)
    segment = lax.all_gather(arrived, "tp", axis=3, tiled=True)
    gate_more = jnp.einsum(
        "secd,edh->sech", segment, gate_served, preferred_element_type=jnp.float32
    )
    up_more = jnp.einsum("secd,edh->sech", segment, up_served, preferred_element_type=jnp.float32)
    input_scale = d_model ** (-0.5)
    hidden = (jax.nn.silu(gate_more * input_scale) * (up_more * input_scale)).astype(jnp.bfloat16)
    hidden_scale = (hidden_local * lax.axis_size("tp")) ** (-0.5)
    slots_here = sources * per_device * capacity
    partial_value = jnp.einsum(
        "edh,sech->dsec", down_served, hidden, preferred_element_type=jnp.float32
    )
    summed = lax.psum_scatter(
        (
            partial_value.reshape(
                lax.axis_size("tp") * (d_model // lax.axis_size("tp")), slots_here
            )
            * hidden_scale
        ).astype(jnp.bfloat16),
        "tp",
        scatter_dimension=0,
        tiled=True,
    )
    returned = lax.all_to_all(summed, "fs", split_axis=1, concat_axis=1, tiled=True)
    picked = jnp.take(returned, slot_index, axis=1).astype(jnp.float32)
    combined = jnp.einsum("dtk,tk->td", picked, route_weights, precision=lax.Precision.HIGHEST)
    return (gate_served, up_served, down_served, combined.astype(jnp.bfloat16))


def solution(mesh):
    placed = (
        P("fs", None),
        P("fs", None),
        P("fs", None),
        P("fs"),
        P(None, "fs", "tp"),
        P(None, "fs", "tp"),
        P(None, "fs", "tp"),
    )
    return jax.shard_map(
        body,
        mesh=mesh,
        in_specs=placed,
        out_specs=(P("fs", None, "tp"), P("fs", None, "tp"), P("fs", None, "tp"), P("fs", "tp")),
        check_vma=False,
    )
```

profile of v0, /device:TPU:0, one launch (start us, length us, event | category | flops | bytes accessed | tf_op | source)
XLA Modules:
  0.0 264.3 jit_solution(7585327871721887649)
XLA Ops:
  7.2 1.1 convert_element_type.43
  8.3 1.2 multiply_reduce_fusion
  9.7 0.1 eq.29
  9.8 0.1 eq.25
  10.0 0.6 reduce-window.6
  10.6 0.2 slice_reduce_fusion
  10.9 0.1 mul.85
  11.3 1.4 scatter_custom_fusion
  12.9 2.6 gather_fusion
  15.5 7.3 %all-to-all-start.3 = ((bf16[8,64,512]{2,1,0:T(8,128)(2,1)}), bf16[8,64,512]{2,1,0:T(8,128)(2,1)S(1)}, u32[]{:S(2)}, u32[]{:S(2)}) async-start(bf16[8,64,512]{2,1,0:T(8,128)(2,1)} %bitcast.15), calls=%async_computation.3 | async-start | bytes 1048576 | tf_op jit(solution)/shard_map/all_to_all | solution.py:43
  22.8 5.8 %multiply_convert_fusion.1 = (bf16[16,256,256]{2,1,0:T(8,128)(2,1)}, bf16[16,256,256]{2,1,0:T(8,128)(2,1)S(1)}) fusion(f32[16,256,256]{2,1,0:T(8,128)} %param.12, f32[256]{0:T(256)S(1)} %copy-done.3, f32[16,256,256]{2,1,0:T(8,128)} %param.11), kind=kLoop, calls=%fused_computation.4 | loop fusion | flops 4194304 | bytes 12583936 | tf_op jit(solution)/shard_map/convert_element_type | solution.py:15
  28.6 8.7 %all-to-all-done.3 = bf16[8,64,512]{2,1,0:T(8,128)(2,1)S(1)} async-done(((bf16[8,64,512]{2,1,0:T(8,128)(2,1)}), bf16[8,64,512]{2,1,0:T(8,128)(2,1)S(1)}, u32[]{:S(2)}, u32[]{:S(2)}) %all-to-all-start.3) | async-done | bytes 524320 | tf_op jit(solution)/shard_map/all_to_all | solution.py:43
  37.3 51.9 %all_to_all.75 = bf16[16,256,256]{2,1,0:T(8,128)(2,1)} all-to-all(bf16[16,256,256]{2,1,0:T(8,128)(2,1)S(1)} %get-tuple-element.7), channel_id=1, replica_groups=mesh['fs'=8,'tp'=4] {'fs'}, dimensions={0} | all-to-all | bytes 4194304 | tf_op jit(solution)/shard_map/all_to_all | solution.py:18
  89.2 4.3 %all-to-all-start.1 = ((bf16[16,256,256]{2,1,0:T(8,128)(2,1)}), bf16[16,256,256]{2,1,0:T(8,128)(2,1)}, u32[]{:S(2)}, u32[]{:S(2)}) async-start(bf16[16,256,256]{2,1,0:T(8,128)(2,1)} %get-tuple-element.6), calls=%async_computation.1 | async-start | bytes 4194304 | tf_op jit(solution)/shard_map/all_to_all | solution.py:19
  93.5 3.8 %convert_element_type.40 = bf16[16,256,256]{2,1,0:T(8,128)(2,1)} convert(f32[16,256,256]{2,1,0:T(8,128)} %param.13) | non-fusion elementwise | flops 1048576 | bytes 6291456 | tf_op jit(solution)/shard_map/convert_element_type | solution.py:16
  97.3 43.5 %all-to-all-done.1 = bf16[16,256,256]{2,1,0:T(8,128)(2,1)} async-done(((bf16[16,256,256]{2,1,0:T(8,128)(2,1)}), bf16[16,256,256]{2,1,0:T(8,128)(2,1)}, u32[]{:S(2)}, u32[]{:S(2)}) %all-to-all-start.1) | async-done | bytes 2097184 | tf_op jit(solution)/shard_map/all_to_all | solution.py:19
  140.8 4.4 %all-to-all-start.2 = ((bf16[16,256,256]{2,1,0:T(8,128)(2,1)}), bf16[16,256,256]{2,1,0:T(8,128)(2,1)}, u32[]{:S(2)}, u32[]{:S(2)}) async-start(bf16[16,256,256]{2,1,0:T(8,128)(2,1)} %convert_element_type.40), calls=%async_computation.2 | async-start | bytes 4194304 | tf_op jit(solution)/shard_map/all_to_all | solution.py:20
  145.2 0.9 copy.33
  146.2 1.5 copy.24
  147.6 3.1 %copy.25 = bf16[8,2,256,256]{3,2,0,1:T(8,128)(2,1)} copy(bf16[8,2,256,256]{3,2,1,0:T(8,128)(2,1)} %bitcast.3) | data formatting | bytes 4194304 | tf_op jit(solution)/shard_map/all_to_all | solution.py:19
  150.7 42.2 %all-to-all-done.2 = bf16[16,256,256]{2,1,0:T(8,128)(2,1)} async-done(((bf16[16,256,256]{2,1,0:T(8,128)(2,1)}), bf16[16,256,256]{2,1,0:T(8,128)(2,1)}, u32[]{:S(2)}, u32[]{:S(2)}) %all-to-all-start.2) | async-done | bytes 2097184 | tf_op jit(solution)/shard_map/all_to_all | solution.py:20
  193.0 3.2 %copy.26 = bf16[8,2,256,256]{3,2,0,1:T(8,128)(2,1)} copy(bf16[8,2,256,256]{3,2,1,0:T(8,128)(2,1)} %bitcast.6) | data formatting | bytes 4194304 | tf_op jit(solution)/shard_map/all_to_all | solution.py:20
  196.2 2.3 fusion.3
  198.5 4.2 %fusion = bf16[2048,8,2,32]{0,3,1,2:T(8,128)(2,1)S(1)} fusion(bf16[2,2048,256,1]{2,1,3,0:T(8,128)(2,1)} %bitcast.82, bf16[2,2048,256,1]{2,1,3,0:T(8,128)(2,1)} %bitcast.80, bf16[8,2,32,2048]{3,2,0,1:T(8,128)(2,1)} %all-gather.2.cloned.1.call-done, f32[8,2,32,256]{3,2,0,1:T(8,128)S(1)} %fusion.3), kind=kOutput, calls=%fused_computation.6 | convolution fusion | flops 1076756480 | bytes 8912896 | tf_op jit(solution)/shard_map/edh,sech->dsec/dot_general | solution.py:54
  202.8 1.5 copy.34
  204.3 30.4 %reduce-scatter.2.cloned.1.call-done = bf16[512,512]{0,1:T(8,128)(2,1)} async-done(((bf16[2048,512]{0,1:T(8,128)(2,1)}), bf16[512,512]{0,1:T(8,128)(2,1)}) %reduce-scatter.2.cloned.1.call-update) | async-done | bytes 524304 | tf_op jit(solution)/shard_map/reduce_scatter | solution.py:57
  234.6 5.5 %all-to-all-start.4 = ((bf16[512,8,64]{0,2,1:T(8,128)(2,1)}), bf16[512,8,64]{0,2,1:T(8,128)(2,1)S(1)}, u32[]{:S(2)}, u32[]{:S(2)}) async-start(bf16[512,8,64]{0,2,1:T(8,128)(2,1)} %bitcast.85), calls=%async_computation.5 | async-start | bytes 1048576 | tf_op jit(solution)/shard_map/all_to_all | solution.py:68
  240.5 0.1 reshape.98
  240.9 13.6 %all-to-all-done.4 = bf16[512,8,64]{0,2,1:T(8,128)(2,1)S(1)} async-done(((bf16[512,8,64]{0,2,1:T(8,128)(2,1)}), bf16[512,8,64]{0,2,1:T(8,128)(2,1)S(1)}, u32[]{:S(2)}, u32[]{:S(2)}) %all-to-all-start.4) | async-done | bytes 524320 | tf_op jit(solution)/shard_map/all_to_all | solution.py:68
  254.5 1.2 gather_fusion.1
  255.8 1.1 fusion.14
  256.8 0.7 copy.44
  (37 shorter events, 1.4 us)
Async XLA Ops:
  7.2 2.4 copy-start.2
  12.8 9.9 %copy-start.3 = (f32[256]{0:T(256)S(1)}, f32[256]{0:T(256)}, u32[]{:S(2)}) copy-start(f32[256]{0:T(256)} %param.10) | copy-start | bytes 3076
  15.5 21.8 %all-to-all-start.3 = ((bf16[8,64,512]{2,1,0:T(8,128)(2,1)}), bf16[8,64,512]{2,1,0:T(8,128)(2,1)S(1)}, u32[]{:S(2)}, u32[]{:S(2)}) async-start(bf16[8,64,512]{2,1,0:T(8,128)(2,1)} %bitcast.15), calls=%async_computation.3 | async-start | bytes 1048576 | tf_op jit(solution)/shard_map/all_to_all | solution.py:43
  89.2 51.6 %all-to-all-start.1 = ((bf16[16,256,256]{2,1,0:T(8,128)(2,1)}), bf16[16,256,256]{2,1,0:T(8,128)(2,1)}, u32[]{:S(2)}, u32[]{:S(2)}) async-start(bf16[16,256,256]{2,1,0:T(8,128)(2,1)} %get-tuple-element.6), calls=%async_computation.1 | async-start | bytes 4194304 | tf_op jit(solution)/shard_map/all_to_all | solution.py:19
  97.3 48.8 %copy-start = (bf16[16,256,256]{2,1,0:T(8,128)(2,1)S(1)}, bf16[16,256,256]{2,1,0:T(8,128)(2,1)}, u32[]{:S(2)}) copy-start(bf16[16,256,256]{2,1,0:T(8,128)(2,1)} %all_to_all.75) | copy-start | bytes 6291460
  140.8 52.2 %all-to-all-start.2 = ((bf16[16,256,256]{2,1,0:T(8,128)(2,1)}), bf16[16,256,256]{2,1,0:T(8,128)(2,1)}, u32[]{:S(2)}, u32[]{:S(2)}) async-start(bf16[16,256,256]{2,1,0:T(8,128)(2,1)} %convert_element_type.40), calls=%async_computation.2 | async-start | bytes 4194304 | tf_op jit(solution)/shard_map/all_to_all | solution.py:20
  145.2 51.0 %all-gather.2.cloned.1.call-start = ((), (), s32[]{:S(2)}) async-start(), calls=%async_computation.6 | async-start | bytes 2621440 | tf_op jit(solution)/shard_map/all_gather | solution.py:45
  146.1 88.5 %reduce-scatter.2.cloned.1.call-start = ((), (), s32[]{:S(2)}) async-start(), calls=%async_computation.7 | async-start | bytes 2621440 | tf_op jit(solution)/shard_map/reduce_scatter | solution.py:57
  193.0 3.3 %copy-start.1 = (bf16[8,2,256,256]{3,2,0,1:T(8,128)(2,1)S(1)}, bf16[8,2,256,256]{3,2,0,1:T(8,128)(2,1)}, u32[]{:S(2)}) copy-start(bf16[8,2,256,256]{3,2,0,1:T(8,128)(2,1)} %copy.24) | copy-start | bytes 6291460
  204.2 36.5 %copy-start.4 = (f32[128,2]{0,1:T(2,128)S(1)}, f32[128,2]{0,1:T(2,128)}, u32[]{:S(2)}) copy-start(f32[128,2]{0,1:T(2,128)} %param.9) | copy-start | bytes 3076
  234.6 19.8 %all-to-all-start.4 = ((bf16[512,8,64]{0,2,1:T(8,128)(2,1)}), bf16[512,8,64]{0,2,1:T(8,128)(2,1)S(1)}, u32[]{:S(2)}, u32[]{:S(2)}) async-start(bf16[512,8,64]{0,2,1:T(8,128)(2,1)} %bitcast.85), calls=%async_computation.5 | async-start | bytes 1048576 | tf_op jit(solution)/shard_map/all_to_all | solution.py:68
Sparse Core Ops, SparseCore 0:
  147.5 23.8 all-gather.1
  204.4 30.2 reduce-scatter.1
where the time goes:
time: 265 us; the launch traced here: 264 us
  waiting for transfers between devices  138 us (52%)
  blocking collectives  51.9 us (20%)
  starting transfers between devices  21.6 us (8%)
  local copies, waits for them, and re-layouts  17.8 us (7%)
  between operations  14.2 us (5%)
  other arithmetic  12.9 us (5%)
  matrix products  7.6 us (3%)
    all_to_all x1, blocking collectives, body(): lax.all_to_all(gate_folded, 'fs', split_axis=0, concat_axis=1, tiled=True)  51.9 us
    all_to_all x1, waiting for transfers between devices, body(): lax.all_to_all(up_folded, 'fs', split_axis=0, concat_axis=1, tiled=True)  43.5 us
    all_to_all x1, waiting for transfers between devices, body(): lax.all_to_all(down_rounded, 'fs', split_axis=0, concat_axis=1, tiled=True)  42.2 us
    reduce_scatter x1, waiting for transfers between devices, body(): lax.psum_scatter((partial_value.reshape(lax.axis_size('tp') * (d_model //...  30.4 us
    all_to_all x1, waiting for transfers between devices, body(): lax.all_to_all(summed, 'fs', split_axis=1, concat_axis=1, tiled=True)  13.6 us
    all_to_all x1, waiting for transfers between devices, body(): lax.all_to_all(own_cols[slot_token], 'fs', split_axis=0, concat_axis=0, t...  8.67 us
    all_to_all x1, starting transfers between devices, body(): lax.all_to_all(own_cols[slot_token], 'fs', split_axis=0, concat_axis=0, t...  7.28 us
    convert_element_type x1, other arithmetic, body(): up_folded = (scaling * up_weight).astype(jnp.bfloat16)  5.81 us
  transfers between devices with their start and end apart: 6, of which 5 were waited for; matrix products, arithmetic and copies ran while one was open for 7% of the time, Pallas kernels for 0%

commit v1 on v0

v1 whole, which is shorter than its diff:
```python
import functools

import jax
import jax.numpy as jnp
from jax import lax
from jax.experimental import pallas as pl
from jax.experimental.pallas import tpu as pltpu
from jax.sharding import PartitionSpec as P

GROUPS = 4
EPSILON = 1e-06
MESH = pl.DeviceIdType.MESH
F32, BF16, I32 = jnp.float32, jnp.bfloat16, jnp.int32


def matmul(a, b, contract=((1,), (0,))):
    return lax.dot_general(a, b, (contract, ((), ())), preferred_element_type=F32)


def kernel(
    nf, nt,
    tokens, ids, ids_t, weights, gain, gate, up, down,
    gate_out, up_out, down_out, combined,
    wf, ws, wr, xs, xr, hs, ps, pr, rs, ret,
    load_sem, wsend, wrecv, xsend, xrecv, gsend, grecv, psend, precv, rsend, rrecv, out_sem,
):
    f, t = lax.axis_index("fs"), lax.axis_index("tp")
    experts, rows, hidden = gate.shape
    n_tok, d_model = tokens.shape
    per = experts // nf
    cap = n_tok * GROUPS // experts
    cols = d_model // nt
    slots = experts * cap
    per_owner = cols // rows
    step = jnp.where(f < nf // 2, 1, nf - 1)

    def peer(k):
        return lax.rem(f + k * step, nf)

    def other(k):
        return lax.rem(t + k, nt)

    def loads(a, k):
        p = peer(k)
        block = pl.ds(p * per, per)
        return pltpu.make_async_copy(
            (gate, up, down)[a].at[block], wf.at[a, block], load_sem.at[a, k]
        )

    def weight_copy(a, p, source):
        return pltpu.make_async_remote_copy(
            src_ref=ws.at[a, pl.ds(p * per, per)],
            dst_ref=wr.at[a, :, pl.ds(pl.multiple_of(source * rows, rows), rows), :],
            send_sem=wsend.at[a, p],
            recv_sem=wrecv.at[a, source],
            device_id={"fs": p},
            device_id_type=MESH,
        )

    def token_copy(p, source):
        return pltpu.make_async_remote_copy(
            src_ref=xs.at[pl.ds(p * per, per)],
            dst_ref=xr.at[t, :, pl.ds(pl.multiple_of(source * cap, cap), cap), :],
            send_sem=xsend.at[p],
            recv_sem=xrecv.at[source],
            device_id={"fs": p},
            device_id_type=MESH,
        )

    def gather_copy(o, source):
        return pltpu.make_async_remote_copy(
            src_ref=xr.at[source],
            dst_ref=xr.at[source],
            send_sem=gsend.at[o],
            recv_sem=grecv.at[source],
            device_id={"tp": o},
            device_id_type=MESH,
        )

    def partial_copy(o, source):
        return pltpu.make_async_remote_copy(
            src_ref=ps.at[o],
            dst_ref=pr.at[source],
            send_sem=psend.at[o],
            recv_sem=precv.at[source],
            device_id={"tp": o},
            device_id_type=MESH,
        )

    def return_copy(p, source):
        return pltpu.make_async_remote_copy(
            src_ref=rs.at[:, pl.ds(pl.multiple_of(p * cap, cap), cap), :],
            dst_ref=ret.at[pl.ds(source * per, per)],
            send_sem=rsend.at[p],
            recv_sem=rrecv.at[source],
            device_id={"fs": p},
            device_id_type=MESH,
        )

    def each(first, last, action):
        def go(k, carry):
            action(k)
            return carry
        lax.fori_loop(first, last, go, 0)

    for a in range(3):
        each(1, nf, lambda k: loads(a, k).start())
        loads(a, 0).start()

    barrier = pltpu.get_barrier_semaphore()
    each(1, nf, lambda k: pl.semaphore_signal(
        barrier, inc=1, device_id={"fs": peer(k)}, device_id_type=MESH))
    each(1, nt, lambda k: pl.semaphore_signal(
        barrier, inc=1, device_id={"tp": other(k)}, device_id_type=MESH))
    pl.semaphore_wait(barrier, nf + nt - 2)

    def converted(a, p):
        value = wf[a, pl.ds(p * per, per)]
        if a < 2:
            value = value * gain[...][None]
        return value.astype(BF16)

    def send_weights(a):
        def one(k):
            p = peer(k)
            loads(a, k).wait()
            ws[a, pl.ds(p * per, per)] = converted(a, p)
            weight_copy(a, p, f).start()
        each(1, nf, one)
        loads(a, 0).wait()
        wr[a, :, pl.ds(pl.multiple_of(f * rows, rows), rows), :] = converted(a, f)

    send_weights(0)

    wide = tokens[...].astype(F32)
    scale = lax.rsqrt(jnp.mean(wide * wide, axis=1, keepdims=True) + EPSILON)
    own = tokens[:, pl.ds(pl.multiple_of(t * cols, cols), cols)].astype(F32)
    normed = (own * scale).astype(BF16)
    slot = lax.broadcasted_iota(I32, (slots, n_tok), 0)
    slot_expert, slot_place = slot // cap, slot % cap
    named = (ids_t[0:1, :] == slot_expert) | (ids_t[1:2, :] == slot_expert)
    earlier = (
        lax.broadcasted_iota(I32, (n_tok, n_tok), 0) < lax.broadcasted_iota(I32, (n_tok, n_tok), 1)
    )
    place = matmul(named.astype(F32).astype(BF16), earlier.astype(F32).astype(BF16))
    chosen = named & (place.astype(I32) == slot_place)
    picked = matmul(chosen.astype(F32).astype(BF16), normed)
    xs[...] = picked.reshape(experts, cap, cols).astype(BF16)
    each(1, nf, lambda k: token_copy(peer(k), f).start())
    own_rows = pl.ds(pl.multiple_of(f * cap, cap), cap)
    xr[t, :, own_rows, :] = xs[pl.ds(f * per, per)]

    send_weights(1)
    send_weights(2)

    each(1, nf, lambda k: token_copy(f, peer(k)).wait_recv())
    each(1, nt, lambda k: gather_copy(other(k), t).start())
    each(1, nt, lambda k: gather_copy(t, other(k)).wait_recv())

    def product(a, e):
        total = jnp.zeros((nf * cap, hidden), F32)
        for o in range(nt):
            total += matmul(xr[o, e], wr[a, e, o * cols:(o + 1) * cols, :])
        return total * d_model ** (-0.5)

    outs = [pltpu.make_async_copy(wr.at[a], (gate_out, up_out, down_out)[a], out_sem.at[a])
            for a in range(3)]
    each(1, nf, lambda k: weight_copy(0, f, peer(k)).wait_recv())
    outs[0].start()
    gates = [product(0, e) for e in range(per)]
    each(1, nf, lambda k: weight_copy(1, f, peer(k)).wait_recv())
    outs[1].start()
    for e in range(per):
        ups = product(1, e)
        v = gates[e]
        hs[e] = (v / (1.0 + jnp.exp(-v)) * ups).astype(BF16)

    hidden_scale = (hidden * nt) ** (-0.5)

    def block(j):
        o = jnp.where(f < nf // 2, j, nt - 1 - j)

        def arrived(i):
            s = o * per_owner + i

            @pl.when(s != f)
            def _():
                weight_copy(2, f, s).wait_recv()
        each(0, per_owner, arrived)
        for e in range(per):
            tile = wr[2, e, pl.ds(pl.multiple_of(o * cols, cols), cols), :]
            part = matmul(hs[e], tile, ((1,), (1,))) * hidden_scale
            ps[o, e] = part.astype(BF16)

        @pl.when(o != t)
        def _():
            partial_copy(o, t).start()
    each(0, nt, block)
    outs[2].start()

    for e in range(per):
        pr[t, e] = ps[t, e]
    each(1, nt, lambda k: partial_copy(t, other(k)).wait_recv())
    for e in range(per):
        total = pr[0, e].astype(F32)
        for o in range(1, nt):
            total += pr[o, e].astype(F32)
        rs[e] = total.astype(BF16)
    each(1, nf, lambda k: return_copy(peer(k), f).start())
    ret[pl.ds(f * per, per)] = rs[:, own_rows, :]

    slot = lax.broadcasted_iota(I32, (n_tok, slots), 1)
    slot_expert, slot_place = slot // cap, slot % cap
    first, second = ids[:, 0:1] == slot_expert, ids[:, 1:2] == slot_expert
    earlier = (
        lax.broadcasted_iota(I32, (n_tok, n_tok), 1) < lax.broadcasted_iota(I32, (n_tok, n_tok), 0)
    )
    place = matmul(earlier.astype(F32).astype(BF16), (first | second).astype(F32).astype(BF16))
    share = jnp.where(first, weights[:, 0:1], jnp.where(second, weights[:, 1:2], 0.0))
    share = jnp.where(place.astype(I32) == slot_place, share, 0.0)
    high = share.astype(BF16)
    low = (share - high.astype(F32)).astype(BF16)
    each(1, nf, lambda k: return_copy(f, peer(k)).wait_recv())
    back = ret[...].astype(F32).reshape(slots, cols).astype(BF16)
    combined[...] = (matmul(high, back) + matmul(low, back)).astype(BF16)

    def drain(k):
        p = peer(k)
        for a in range(3):
            weight_copy(a, p, f).wait_send()
        token_copy(p, f).wait_send()
        return_copy(p, f).wait_send()
    each(1, nf, drain)

    def drain_tp(k):
        gather_copy(other(k), t).wait_send()
        partial_copy(other(k), t).wait_send()
    each(1, nt, drain_tp)
    for copy in outs:
        copy.wait()


def body(nf, nt, tokens, route_ids, route_weights, norm_gain, gate_weight, up_weight, down_weight):
    experts, rows, hidden = gate_weight.shape
    n_tok, d_model = tokens.shape
    per = experts // nf
    cap = n_tok * GROUPS // experts
    cols = d_model // nt
    served = jax.ShapeDtypeStruct((per, nf * rows, hidden), BF16)
    vmem, anywhere = pl.BlockSpec(memory_space=pltpu.VMEM), pl.BlockSpec(memory_space=pl.ANY)
    dma = pltpu.SemaphoreType.DMA
    return pl.pallas_call(
        functools.partial(kernel, nf, nt),
        out_shape=(served, served, served, jax.ShapeDtypeStruct((n_tok, cols), BF16)),
        in_specs=[vmem] * 5 + [anywhere] * 3,
        out_specs=(anywhere, anywhere, anywhere, vmem),
        scratch_shapes=[
            pltpu.VMEM((3, experts, rows, hidden), F32),
            pltpu.VMEM((3, experts, rows, hidden), BF16),
            pltpu.VMEM((3, per, nf * rows, hidden), BF16),
            pltpu.VMEM((experts, cap, cols), BF16),
            pltpu.VMEM((nt, per, nf * cap, cols), BF16),
            pltpu.VMEM((per, nf * cap, hidden), BF16),
            pltpu.VMEM((nt, per, nf * cap, cols), BF16),
            pltpu.VMEM((nt, per, nf * cap, cols), BF16),
            pltpu.VMEM((per, nf * cap, cols), BF16),
            pltpu.VMEM((experts, cap, cols), BF16),
            dma((3, nf)),
            dma((3, nf)), dma((3, nf)),
            dma((nf,)), dma((nf,)),
            dma((nt,)), dma((nt,)),
            dma((nt,)), dma((nt,)),
            dma((nf,)), dma((nf,)),
            dma((3,)),
        ],
        compiler_params=pltpu.CompilerParams(
            collective_id=0, has_side_effects=True, vmem_limit_bytes=56 * 1024 * 1024
        ),
    )(
        tokens, route_ids, route_ids.T, route_weights, norm_gain[:, None],
        gate_weight, up_weight, down_weight,
    )


def solution(mesh):
    split = P(None, "fs", "tp")
    served = P("fs", None, "tp")
    return jax.shard_map(
        functools.partial(body, mesh.shape["fs"], mesh.shape["tp"]),
        mesh=mesh,
        in_specs=(P("fs", None), P("fs", None), P("fs", None), P("fs"), split, split, split),
        out_specs=(served, served, served, P("fs", "tp")),
        check_vma=False,
    )
```

time: 265 us -> 203 us (0.77)
  Pallas kernels: 0 us -> 190 us
  waiting for transfers between devices: 138 us -> 0 us
  blocking collectives: 51.9 us -> 0 us
  starting transfers between devices: 21.6 us -> 0 us
  between operations: 14.2 us -> 0.65 us
  other arithmetic: 12.9 us -> 0 us
  matrix products: 7.6 us -> 0 us
  local copies, waits for them, and re-layouts: 17.8 us -> 11.8 us
    pallas_call x0 -> x1, Pallas kernels: none -> 190 us  [body(): pl.pallas_call(functools.partial(kernel, nf, nt), out_shape=(served, serv...]
    all_to_all x4 -> x0, waiting for transfers between devices: 108 us -> none  [the longest x1 43.5 us: body(): lax.all_to_all(up_folded, 'fs', split_axis=0, concat_axis=1, tiled=True)]
    all_to_all x1 -> x0, blocking collectives: 51.9 us -> none  [body(): lax.all_to_all(gate_folded, 'fs', split_axis=0, concat_axis=1, tiled=True)]
    reduce_scatter x1 -> x0, waiting for transfers between devices: 30.4 us -> none  [body(): lax.psum_scatter((partial_value.reshape(lax.axis_size('tp') * (d_model //...]
    all_to_all x4 -> x0, starting transfers between devices: 21.5 us -> none  [the longest x1 7.28 us: body(): lax.all_to_all(own_cols[slot_token], 'fs', split_axis=0, concat_axis=0, t...]
    convert_element_type x5 -> x0, other arithmetic: 10.9 us -> none  [the longest x1 5.81 us: body(): up_folded = (scaling * up_weight).astype(jnp.bfloat16)]
    unnamed x12, local copies, waits for them, and re-layouts: 0.25 us -> 10.3 us
    all_to_all x3 -> x0, local copies, waits for them, and re-layouts: 7.8 us -> none  [the longest x1 3.24 us: body(): lax.all_to_all(down_rounded, 'fs', split_axis=0, concat_axis=1, tiled=True)]
  transfers between devices with their start and end apart: 6 -> 0, of which waited for: 5 -> 0; matrix products, arithmetic and copies ran while one was open for 7% -> 0% of each run, Pallas kernels for 0% -> 0%
where the time goes in v1:
time: 203 us
  Pallas kernels  190 us (94%)
  local copies, waits for them, and re-layouts  11.8 us (6%)
    pallas_call x1, Pallas kernels, body(): pl.pallas_call(functools.partial(kernel, nf, nt), out_shape=(served, serv...  190 us
    unnamed x12, local copies, waits for them, and re-layouts  10.3 us

profile of v1, /device:TPU:0, one launch (start us, length us, event | category | flops | bytes accessed | tf_op | source)
XLA Modules:
  0.0 202.9 jit_solution(5987592989591282278)
XLA Ops:
  0.6 1.4 copy.14.weights
  2.0 1.4 copy.13.ids
  3.5 1.5 copy.15.gain
  4.9 190.4 %shard_map.102 = (bf16[2,2048,256]{2,1,0:T(8,128)(2,1)}, bf16[2,2048,256]{2,1,0:T(8,128)(2,1)}, bf16[2,2048,256]{2,1,0:T(8,128)(2,1)}, bf16[128,512]{1,0:T(8,128)(2,1)}) custom-call(bf16[128,2048]{1,0:T(8,128)(2,1)} %tokens.1, s32[128,2]{1,0:T(8,128)} %copy.13.ids, s32[2,128]{1,0:T(2,128)} %bitcast.2, f32[128,2]{1,0:T(8,128)} %copy.14.weights, ...), custom_call_target="tpu_custom_call" | custom-call | tf_op jit(solution)/shard_map/pallas_call | solution.py:252
  195.3 0.0 copy-start.1
  195.4 3.2 %copy.20 = bf16[2,2048,256]{2,1,0:T(8,128)(2,1)} copy(bf16[2,2048,256]{2,1,0:T(8,128)(2,1)} %get-tuple-element.8) | data formatting | bytes 4194304
  198.6 0.0 copy-done.1
  198.6 0.0 copy-start
  198.6 1.3 copy.21
  199.9 1.0 copy-done
  200.9 0.0 copy-start.2
  200.9 1.3 copy.22
  202.2 0.0 copy-done.2
  202.2 0.7 copy.23
Async XLA Ops:
  195.3 3.2 %copy-start.1 = (bf16[2,2048,256]{2,1,0:T(8,128)(2,1)S(1)}, bf16[2,2048,256]{2,1,0:T(8,128)(2,1)}, u32[]{:S(2)}) copy-start(bf16[2,2048,256]{2,1,0:T(8,128)(2,1)} %get-tuple-element.9) | copy-start | bytes 6291460
  198.6 2.3 %copy-start = (bf16[2,2048,256]{2,1,0:T(8,128)(2,1)S(1)}, bf16[2,2048,256]{2,1,0:T(8,128)(2,1)}, u32[]{:S(2)}) copy-start(bf16[2,2048,256]{2,1,0:T(8,128)(2,1)} %get-tuple-element.10) | copy-start | bytes 6291460
  200.9 1.3 copy-start.2

commit v2 on v1

v2 whole, which is shorter than its diff:
```python
import functools

import jax
import jax.numpy as jnp
from jax import lax
from jax.experimental import pallas as pl
from jax.experimental.pallas import tpu as pltpu
from jax.sharding import PartitionSpec as P

GROUPS = 4
EPSILON = 1e-06
MESH = pl.DeviceIdType.MESH
LAG = 2
F32, BF16, I32 = jnp.float32, jnp.bfloat16, jnp.int32


def matmul(a, b, contract=((1,), (0,))):
    return lax.dot_general(a, b, (contract, ((), ())), preferred_element_type=F32)


def assignment(ids_t, experts, cap):
    n_tok = ids_t.shape[1]
    slot = lax.broadcasted_iota(I32, (experts * cap, n_tok), 0)
    first, second = ids_t[0:1, :] == slot // cap, ids_t[1:2, :] == slot // cap
    earlier = (
        lax.broadcasted_iota(I32, (n_tok, n_tok), 0) < lax.broadcasted_iota(I32, (n_tok, n_tok), 1)
    )
    named = (first | second).astype(F32).astype(BF16)
    place = matmul(named, earlier.astype(F32).astype(BF16))
    return (first | second) & (place.astype(I32) == slot % cap), first


def kernel(
    nf, nt,
    tokens, ids_t, gain, gate, up, down,
    gate_out, up_out, down_out, ret,
    wf, ws, xs, xr, hs, ps, pr, rs,
    load_sem, wsend, wrecv, xsend, xrecv, gsend, grecv, psend, precv, rsend, rrecv,
):
    f, t = lax.axis_index("fs"), lax.axis_index("tp")
    experts, rows, hidden = gate.shape
    n_tok, d_model = tokens.shape
    per = experts // nf
    cap = n_tok * GROUPS // experts
    cols = d_model // nt
    slots = experts * cap
    per_owner = cols // rows
    served = (gate_out, up_out, down_out)
    low_half = f < nf // 2

    def peer(k):
        down_to = jnp.where(k < nf - f, nf - k, nf - 1 - k)
        up_to = jnp.where(k <= f, k - 1, k)
        return jnp.where(k == 0, f, jnp.where(low_half, down_to, up_to))

    def other(k):
        return lax.rem(t + k, nt)

    def loads(e, a, k):
        n = peer(k) * per + e
        return pltpu.make_async_copy(
            (gate, up, down)[a].at[n], wf.at[a, n], load_sem.at[e, a, k]
        )

    def weight_copy(e, a, p, source):
        return pltpu.make_async_remote_copy(
            src_ref=ws.at[a, p * per + e],
            dst_ref=served[a].at[e, pl.ds(pl.multiple_of(source * rows, rows), rows), :],
            send_sem=wsend.at[e, a, p],
            recv_sem=wrecv.at[e, a, source],
            device_id={"fs": p},
            device_id_type=MESH,
        )

    def token_copy(p, source):
        return pltpu.make_async_remote_copy(
            src_ref=xs.at[pl.ds(p * per, per)],
            dst_ref=xr.at[t, :, pl.ds(pl.multiple_of(source * cap, cap), cap), :],
            send_sem=xsend.at[p],
            recv_sem=xrecv.at[source],
            device_id={"fs": p},
            device_id_type=MESH,
        )

    def gather_copy(o, source):
        return pltpu.make_async_remote_copy(
            src_ref=xr.at[source],
            dst_ref=xr.at[source],
            send_sem=gsend.at[o],
            recv_sem=grecv.at[source],
            device_id={"tp": o},
            device_id_type=MESH,
        )

    def partial_copy(e, s, source):
        return pltpu.make_async_remote_copy(
            src_ref=ps.at[e, s],
            dst_ref=pr.at[source, e, lax.rem(s, per_owner)],
            send_sem=psend.at[e, s],
            recv_sem=precv.at[source, e, lax.rem(s, per_owner)],
            device_id={"tp": s // per_owner},
            device_id_type=MESH,
        )

    def return_copy(e, p, source, i):
        return pltpu.make_async_remote_copy(
            src_ref=rs.at[e, i, pl.ds(pl.multiple_of(p * cap, cap), cap), :],
            dst_ref=ret.at[i, source * per + e],
            send_sem=rsend.at[e, i, p],
            recv_sem=rrecv.at[e, i, source],
            device_id={"fs": p},
            device_id_type=MESH,
        )

    def each(first, last, action):
        def go(k, carry):
            action(k)
            return carry
        lax.fori_loop(first, last, go, 0)

    each(1, nf, lambda k: loads(0, 0, k).start())
    loads(0, 0, 0).start()

    barrier = pltpu.get_barrier_semaphore()
    each(1, nf, lambda k: pl.semaphore_signal(
        barrier, inc=1, device_id={"fs": peer(k)}, device_id_type=MESH))
    each(1, nt, lambda k: pl.semaphore_signal(
        barrier, inc=1, device_id={"tp": other(k)}, device_id_type=MESH))
    pl.semaphore_wait(barrier, nf + nt - 2)

    square = lax.broadcasted_iota(I32, (rows, rows), 0) == lax.broadcasted_iota(I32, (rows, rows), 1)
    gain_column = jnp.sum(jnp.where(square, gain[...], 0.0), axis=1, keepdims=True)

    def converted(a, n):
        value = wf[a, n]
        if a < 2:
            value = value * gain_column
        return value.astype(BF16)

    def send_weights(e, a):
        e_next, a_next = (e, a + 1) if a < 2 else (e + 1, 0)

        def load_next(k):
            if e_next < per:
                loads(e_next, a_next, k).start()

        def one(k):
            p = peer(k)
            loads(e, a, k).wait()
            load_next(k)
            ws[a, p * per + e] = converted(a, p * per + e)
            weight_copy(e, a, p, f).start()
        each(1, nf, one)
        loads(e, a, 0).wait()
        load_next(0)
        served[a][e, pl.ds(pl.multiple_of(f * rows, rows), rows), :] = converted(a, f * per + e)

    send_weights(0, 0)

    wide = tokens[...].astype(F32)
    scale = lax.rsqrt(jnp.mean(wide * wide, axis=1, keepdims=True) + EPSILON)
    own = tokens[:, pl.ds(pl.multiple_of(t * cols, cols), cols)].astype(F32)
    normed = (own * scale).astype(BF16)
    chosen, _ = assignment(ids_t, experts, cap)
    picked = matmul(chosen.astype(F32).astype(BF16), normed)
    xs[...] = picked.reshape(experts, cap, cols).astype(BF16)
    each(1, nf, lambda k: token_copy(peer(k), f).start())
    own_rows = pl.ds(pl.multiple_of(f * cap, cap), cap)
    xr[t, :, own_rows, :] = xs[pl.ds(f * per, per)]

    for e in range(per):
        for a in range(3):
            if e + a > 0:
                send_weights(e, a)

    each(1, nf, lambda k: token_copy(f, peer(k)).wait_recv())
    each(1, nt, lambda k: gather_copy(other(k), t).start())
    each(1, nt, lambda k: gather_copy(t, other(k)).wait_recv())

    def product(a, e):
        total = jnp.zeros((nf * cap, hidden), F32)
        for o in range(nt):
            total += matmul(xr[o, e], served[a][e, o * cols:(o + 1) * cols, :])
        return total * d_model ** (-0.5)

    hidden_scale = (hidden * nt) ** (-0.5)

    def block_at(j):
        return jnp.where(low_half, j, nf - 1 - j)

    def block(e, j):
        s = block_at(j)

        @pl.when(s != f)
        def _():
            weight_copy(e, 2, f, s).wait_recv()
        tile = down_out[e, pl.ds(pl.multiple_of(s * rows, rows), rows), :]
        ps[e, s] = (matmul(hs[...], tile, ((1,), (1,))) * hidden_scale).astype(BF16)

        @pl.when(s // per_owner != t)
        def _():
            partial_copy(e, s, t).start()

    def finish(e, j):
        s = block_at(j)
        i = lax.rem(s, per_owner)

        @pl.when(s // per_owner == t)
        def _():
            each(1, nt, lambda k: partial_copy(e, s, other(k)).wait_recv())
            total = ps[e, s].astype(F32)
            for k in range(1, nt):
                total += pr[other(k), e, i].astype(F32)
            rs[e, i] = total.astype(BF16)
            each(1, nf, lambda k: return_copy(e, peer(k), f, i).start())
            ret[i, f * per + e] = rs[e, i, own_rows, :]

    for e in range(per):
        each(1, nf, lambda k: weight_copy(e, 0, f, peer(k)).wait_recv())
        v = product(0, e)
        each(1, nf, lambda k: weight_copy(e, 1, f, peer(k)).wait_recv())
        hs[...] = (v / (1.0 + jnp.exp(-v)) * product(1, e)).astype(BF16)

        each(0, LAG, lambda j: block(e, j))

        def both(j):
            block(e, j)
            finish(e, j - LAG)
        each(LAG, nf, both)
        each(nf - LAG, nf, lambda j: finish(e, j))
    for e in range(per):
        each(0, per_owner, lambda i: each(
            1, nf, lambda k: return_copy(e, f, peer(k), i).wait_recv()))

    def drain(k):
        p = peer(k)
        for e in range(per):
            for a in range(3):
                weight_copy(e, a, p, f).wait_send()
            each(0, per_owner, lambda i: return_copy(e, p, f, i).wait_send())
        token_copy(p, f).wait_send()
    each(1, nf, drain)
    each(1, nt, lambda k: gather_copy(other(k), t).wait_send())

    def drain_partial(s):
        @pl.when(s // per_owner != t)
        def _():
            for e in range(per):
                partial_copy(e, s, t).wait_send()
    each(0, nf, drain_partial)


def finish_kernel(
    ids_t, weights_t, ret, gate, up, down, gate_out, up_out, down_out, combined, sem
):
    outs = [
        pltpu.make_async_copy(source, target, sem.at[a])
        for a, (source, target) in enumerate(((gate, gate_out), (up, up_out), (down, down_out)))
    ]
    for copy in outs:
        copy.start()
    chunks, experts, cap, width = ret.shape
    chosen, first = assignment(ids_t, experts, cap)
    share = jnp.where(chosen, jnp.where(first, weights_t[0:1, :], weights_t[1:2, :]), 0.0).T
    high = share.astype(BF16)
    low = (share - high.astype(F32)).astype(BF16)
    for i in range(chunks):
        back = ret[i].astype(F32).reshape(experts * cap, width).astype(BF16)
        value = matmul(high, back) + matmul(low, back)
        combined[:, i * width:(i + 1) * width] = value.astype(BF16)
    for copy in outs:
        copy.wait()


def body(nf, nt, tokens, route_ids, route_weights, norm_gain, gate_weight, up_weight, down_weight):
    experts, rows, hidden = gate_weight.shape
    n_tok, d_model = tokens.shape
    per = experts // nf
    cap = n_tok * GROUPS // experts
    cols = d_model // nt
    shape = (per, nf * rows, hidden)
    vmem, anywhere = pl.BlockSpec(memory_space=pltpu.VMEM), pl.BlockSpec(memory_space=pl.ANY)
    dma = pltpu.SemaphoreType.DMA
    per_owner = cols // rows
    ids_t, weights_t = route_ids.T, route_weights.T
    *served, ret = pl.pallas_call(
        functools.partial(kernel, nf, nt),
        out_shape=[pltpu.VMEM(shape, BF16)] * 3 + [pltpu.VMEM((per_owner, experts, cap, rows), BF16)],
        in_specs=[vmem] * 3 + [anywhere] * 3,
        out_specs=[vmem] * 4,
        scratch_shapes=[
            pltpu.VMEM((3, experts, rows, hidden), F32),
            pltpu.VMEM((3, experts, rows, hidden), BF16),
            pltpu.VMEM((experts, cap, cols), BF16),
            pltpu.VMEM((nt, per, nf * cap, cols), BF16),
            pltpu.VMEM((nf * cap, hidden), BF16),
            pltpu.VMEM((per, nf, nf * cap, rows), BF16),
            pltpu.VMEM((nt, per, per_owner, nf * cap, rows), BF16),
            pltpu.VMEM((per, per_owner, nf * cap, rows), BF16),
            dma((per, 3, nf)),
            dma((per, 3, nf)), dma((per, 3, nf)),
            dma((nf,)), dma((nf,)),
            dma((nt,)), dma((nt,)),
            dma((per, nf)), dma((nt, per, per_owner)),
            dma((per, per_owner, nf)), dma((per, per_owner, nf)),
        ],
        compiler_params=pltpu.CompilerParams(
            collective_id=0, has_side_effects=True, vmem_limit_bytes=54 * 1024 * 1024
        ),
    )(tokens, ids_t, norm_gain[None, :], gate_weight, up_weight, down_weight)
    out = jax.ShapeDtypeStruct(shape, BF16)
    return pl.pallas_call(
        finish_kernel,
        out_shape=(out, out, out, jax.ShapeDtypeStruct((n_tok, cols), BF16)),
        in_specs=[vmem] * 6,
        out_specs=(anywhere, anywhere, anywhere, vmem),
        scratch_shapes=[dma((3,))],
        compiler_params=pltpu.CompilerParams(vmem_limit_bytes=16 * 1024 * 1024),
    )(ids_t, weights_t, ret, *served)


def solution(mesh):
    split = P(None, "fs", "tp")
    served = P("fs", None, "tp")
    return jax.shard_map(
        functools.partial(body, mesh.shape["fs"], mesh.shape["tp"]),
        mesh=mesh,
        in_specs=(P("fs", None), P("fs", None), P("fs", None), P("fs"), split, split, split),
        out_specs=(served, served, served, P("fs", "tp")),
        check_vma=False,
    )
```

time: 203 us -> 182 us (0.90)
  local copies, waits for them, and re-layouts: 11.8 us -> 0.01 us
  Pallas kernels: 190 us -> 181 us
    unnamed x12 -> x4, local copies, waits for them, and re-layouts: 10.3 us -> 0.01 us
    pallas_call x1 -> x2, Pallas kernels: 190 us -> 181 us  [the longest x1 177 us: body(): pl.pallas_call(functools.partial(kernel, nf, nt), out_shape=[pltpu.VMEM(s...]
where the time goes in v2:
time: 182 us
  Pallas kernels  181 us (99%)
    pallas_call x1, Pallas kernels, body(): pl.pallas_call(functools.partial(kernel, nf, nt), out_shape=[pltpu.VMEM(s...  177 us

profile of v2, /device:TPU:0, one launch (start us, length us, event | category | flops | bytes accessed | tf_op | source)
XLA Modules:
  0.0 181.6 jit_solution(17435238188639039778)
XLA Ops:
  0.6 0.0 copy-start
  0.6 0.0 copy-start.1
  0.7 177.5 %shard_map.102 = (bf16[2,2048,256]{2,1,0:T(8,128)(2,1)S(1)}, bf16[2,2048,256]{2,1,0:T(8,128)(2,1)S(1)}, bf16[2,2048,256]{2,1,0:T(8,128)(2,1)S(1)}, bf16[2,16,32,256]{3,2,1,0:T(8,128)(2,1)S(1)}) custom-call(bf16[128,2048]{1,0:T(8,128)(2,1)} %tokens.1, s32[2,128]{1,0:T(2,128)} %bitcast.3, f32[1,256]{1,0:T(1,128)} %bitcast.6, f32[16,256,256]{2,1,0:T(8,128)} %gate.1, ...), custom_call_target="tpu_custom_call" | custom-call | tf_op jit(solution)/shard_map/pallas_call | solution.py:286
  178.1 0.0 copy-done
  178.2 0.0 copy-done.1
  178.2 3.5 %shard_map.103 = (bf16[2,2048,256]{2,1,0:T(8,128)(2,1)}, bf16[2,2048,256]{2,1,0:T(8,128)(2,1)}, bf16[2,2048,256]{2,1,0:T(8,128)(2,1)}, bf16[128,512]{1,0:T(8,128)(2,1)}) custom-call(s32[2,128]{1,0:T(2,128)S(1)} %bitcast.4, f32[2,128]{1,0:T(2,128)S(1)} %bitcast.5, bf16[2,16,32,256]{3,2,1,0:T(8,128)(2,1)S(1)} %get-tuple-element.8.ret, ...), custom_call_target="tpu_custom_call" | custom-call | tf_op jit(solution)/shard_map/pallas_call | solution.py:312
Async XLA Ops:
  0.6 177.5 %copy-start = (s32[128,2]{0,1:T(2,128)S(1)}, s32[128,2]{0,1:T(2,128)}, u32[]{:S(2)}) copy-start(s32[128,2]{0,1:T(2,128)} %param.8) | copy-start | bytes 3076
  0.6 177.5 %copy-start.1 = (f32[128,2]{0,1:T(2,128)S(1)}, f32[128,2]{0,1:T(2,128)}, u32[]{:S(2)}) copy-start(f32[128,2]{0,1:T(2,128)} %param.9) | copy-start | bytes 3076
